TPU v7x, 32 devices: a whole 2x2x4 slice. The times are simulated.
32 devices in a mesh: ep: 16 (over z, y, x), tp: 2 (over core).
Axes of the slice: x: 2, y: 2, z: 4, core: 2. Of those that a mesh axis runs over, the one named last changes fastest.
Arguments:
- tokens: bfloat16 [64, 4096], P('ep'), may hold values from -6 to 6
- memory: float32 [64, 8, 256, 512], P('ep', 'tp'), may hold values from -6 to 6
- normalizer: float32 [64, 8, 256], P('ep', 'tp'), may hold values from -6 to 6
- stabilizer: float32 [64, 8], P('ep', 'tp'), may hold values from -4 to 4
- norm_gain: float32 [4096], replicated, may hold values from 0.1 to 1.9
- w_query: bfloat16 [4096, 8, 256], P(None, 'tp', 'ep'), may hold values from -0.09375 to 0.09375
- w_key: bfloat16 [4096, 8, 256], P(None, 'tp', 'ep'), may hold values from -0.09375 to 0.09375
- w_value: bfloat16 [4096, 8, 512], P(None, 'tp', 'ep'), may hold values from -0.09375 to 0.09375
- w_outgate: bfloat16 [4096, 8, 512], P(None, 'tp', 'ep'), may hold values from -0.09375 to 0.09375
- w_input: bfloat16 [4096, 8], P(None, 'tp'), may hold values from -0.09375 to 0.09375
- w_forget: bfloat16 [4096, 8], P(None, 'tp'), may hold values from -0.09375 to 0.09375
- forget_bias: float32 [8], P('tp'), may hold values from 0 to 4
- w_out: bfloat16 [4096, 4096], P('tp', 'ep'), may hold values from -0.09375 to 0.09375
- ffn_gain: float32 [4096], replicated, may hold values from 0.1 to 1.9
- w_gate: bfloat16 [16, 4096, 512], P('ep', None, 'tp'), may hold values from -0.09375 to 0.09375
- w_up: bfloat16 [16, 4096, 512], P('ep', None, 'tp'), may hold values from -0.09375 to 0.09375
- w_down: bfloat16 [16, 512, 4096], P('ep', 'tp'), may hold values from -0.25 to 0.25
- expert_ids: int32 [64, 2], P('ep'), may hold values from 0 to 15, as said below
- route_weights: float32 [64, 2], P('ep'), may hold values from 0.1 to 1
Outputs:
- out: bfloat16 [64, 4096], P('ep')
- memory_next: float32 [64, 8, 256, 512], P('ep', 'tp')
- normalizer_next: float32 [64, 8, 256], P('ep', 'tp')
- stabilizer_next: float32 [64, 8], P('ep', 'tp')
Inputs may be any that keep to these rules, and one draw needn't show every extreme that they name: `expert_ids`: the 2 experts of a token differ and lie in one group of 8 consecutive experts. Beyond that, any choice is allowed: for instance, all 4 tokens of one index of ep may name the same expert.
All inputs are finite; a program needn't handle non-finite values.
Results may differ from a plain program's by a relative error of at most 0.013.
Values may be sent and summed in bfloat16 or wider, within the bound.
No kernel may reach another device: no remote copies, remote signals or barrier semaphores. Data moves between devices by JAX's collectives and lax.ppermute only.
A program may use at most 128 MiB of HBM per device.

v0:
```python
import jax
import jax.numpy as jnp
from jax import lax
from jax.sharding import PartitionSpec as P


def rms_scale(values, gain):
    return values * lax.rsqrt(jnp.mean(values * values, axis=-1, keepdims=True) + 1e-06) * gain


def product(left, right):
    return jnp.dot(left, right, preferred_element_type=jnp.float32)


def rounded_term(values):
    return lax.optimization_barrier(values.astype(jnp.bfloat16)).astype(jnp.float32)


def body(
    tokens,
    memory,
    normalizer,
    stabilizer,
    norm_gain,
    w_query,
    w_key,
    w_value,
    w_outgate,
    w_input,
    w_forget,
    forget_bias,
    w_out,
    ffn_gain,
    w_gate,
    w_up,
    w_down,
    expert_ids,
    route_weights,
):
    seqs, width = tokens.shape
    heads, key_size, value_size = (memory.shape[1], memory.shape[2], memory.shape[3])
    value_width = heads * value_size
    key_piece = w_query.shape[2]
    value_piece = w_value.shape[2]
    query_cols = w_query.reshape(width, heads * key_piece)
    key_cols = w_key.reshape(width, heads * key_piece)
    value_cols = w_value.reshape(width, heads * value_piece)
    outgate_cols = w_outgate.reshape(width, heads * value_piece)
    normed = rms_scale(tokens.astype(jnp.float32), norm_gain).astype(jnp.bfloat16)
    piece = lax.all_gather(normed, "ep", axis=0, tiled=True)
    projected = jnp.concatenate(
        [
            product(piece, query_cols),
            product(piece, key_cols),
            product(piece, value_cols),
            product(piece, outgate_cols),
        ],
        axis=1,
    ).astype(jnp.bfloat16)
    all_rows = projected.shape[0]
    narrow = heads * key_piece
    broad = heads * value_piece
    query_part = projected[:, :narrow].reshape(all_rows, heads, key_piece)
    key_part = projected[:, narrow : 2 * narrow].reshape(all_rows, heads, key_piece)
    value_part = projected[:, 2 * narrow : 2 * narrow + broad].reshape(all_rows, heads, value_piece)
    outgate_part = projected[:, 2 * narrow + broad :].reshape(all_rows, heads, value_piece)
    query, key, value, outgate = (
        lax.all_to_all(query_part, "ep", split_axis=0, concat_axis=2, tiled=True),
        lax.all_to_all(key_part, "ep", split_axis=0, concat_axis=2, tiled=True),
        lax.all_to_all(value_part, "ep", split_axis=0, concat_axis=2, tiled=True),
        lax.all_to_all(outgate_part, "ep", split_axis=0, concat_axis=2, tiled=True),
    )
    in_pre = product(normed, w_input)
    log_forget = jax.nn.log_sigmoid(product(normed, w_forget) + forget_bias)
    scaled = query.astype(jnp.float32) * key_size ** (-0.5)
    key_heads = key.astype(jnp.float32)
    value_heads = value.astype(jnp.float32)
    stab_next = jnp.maximum(log_forget + stabilizer, in_pre)
    decay = jnp.exp(log_forget + stabilizer - stab_next)
    inweight = jnp.exp(in_pre - stab_next)
    memory_next = decay[:, :, None, None] * memory + inweight[:, :, None, None] * (
        key_heads[:, :, :, None] * value_heads[:, :, None, :]
    )
    normalizer_next = decay[:, :, None] * normalizer + inweight[:, :, None] * key_heads
    numerator = jnp.einsum("shd,shde->she", scaled, memory_next, precision=lax.Precision.HIGHEST)
    denominator = jnp.sum(scaled * normalizer_next, axis=-1)
    hidden = numerator / jnp.maximum(jnp.abs(denominator), jnp.exp(-stab_next))[:, :, None]
    hidden = (
        hidden.reshape(seqs, value_width)
        * jax.nn.sigmoid(outgate.reshape(seqs, value_width).astype(jnp.float32))
    ).astype(jnp.bfloat16)
    partial_value = product(lax.all_gather(hidden, "ep", axis=0, tiled=True), w_out)
    summed = lax.psum(rounded_term(partial_value).astype(jnp.bfloat16), "tp")
    mixed = lax.all_to_all(summed, "ep", split_axis=0, concat_axis=1, tiled=True)
    resid = tokens.astype(jnp.float32) + mixed.astype(jnp.float32)
    ffn_in = rms_scale(resid, ffn_gain).astype(jnp.bfloat16)
    gate_local, up_local, down_local = (w_gate[0], w_up[0], w_down[0])
    n_experts = lax.axis_size("ep") * w_gate.shape[0]
    piece = lax.all_gather(ffn_in, "ep", axis=0, tiled=True)
    gate_part = product(piece, gate_local)
    up_part = product(piece, up_local)
    act = (jax.nn.silu(gate_part) * up_part).astype(jnp.bfloat16)
    expert_terms = rounded_term(product(act, down_local))
    labels = jnp.arange(n_experts, dtype=jnp.int32)
    route_dense = jnp.sum(
        jnp.where(expert_ids[:, :, None] == labels[None, None, :], route_weights[:, :, None], 0.0),
        axis=1,
    )
    my_weight = lax.all_to_all(route_dense, "ep", split_axis=1, concat_axis=0, tiled=True)
    contrib = expert_terms * my_weight
    n_ep = lax.axis_size("ep")
    n_tp = lax.axis_size("tp")
    arranged = jnp.swapaxes(contrib.reshape(n_ep, seqs, n_tp, width // n_tp), 1, 2)
    arranged = arranged.reshape(n_ep * n_tp * seqs, width // n_tp)
    mine = lax.psum_scatter(arranged, ("ep", "tp"), scatter_dimension=0, tiled=True)
    ffn_out = lax.all_gather(mine.astype(jnp.bfloat16), "tp", axis=1, tiled=True).astype(mine.dtype)
    out = (resid + ffn_out).astype(jnp.bfloat16)
    return (out, memory_next, normalizer_next, stab_next)


def solution(mesh):
    return jax.shard_map(
        body,
        mesh=mesh,
        in_specs=(
            P("ep", None),
            P("ep", "tp", None, None),
            P("ep", "tp", None),
            P("ep", "tp"),
            P(),
            P(None, "tp", "ep"),
            P(None, "tp", "ep"),
            P(None, "tp", "ep"),
            P(None, "tp", "ep"),
            P(None, "tp"),
            P(None, "tp"),
            P("tp"),
            P("tp", "ep"),
            P(),
            P("ep", None, "tp"),
            P("ep", None, "tp"),
            P("ep", "tp", None),
            P("ep", None),
            P("ep", None),
        ),
        out_specs=(P("ep", None), P("ep", "tp", None, None), P("ep", "tp", None), P("ep", "tp")),
        check_vma=False,
    )
```

profile of v0, /device:TPU:0, one launch (start us, length us, event | category | flops | bytes accessed | tf_op | source)
XLA Modules:
  0.0 274.0 jit_solution(16929384175384432204)
XLA Ops:
  2.6 45.3 %all-gather = bf16[16,4,4096]{2,1,0:T(4,128)(2,1)S(1)} all-gather(bf16[1,4,4096]{2,1,0:T(4,128)(2,1)S(1)} %fusion.49), channel_id=1, replica_groups=mesh['ep'=16,'tp'=2] {'ep'}, dimensions={0}, use_global_device_ids=true | all-gather | bytes 557056 | tf_op jit(solution)/shard_map/all_gather | solution.py:50
  50.3 3.5 %all-to-all-start.1 = ((bf16[16,2,128]{2,1,0:T(2,128)(2,1)}), bf16[16,2,128]{2,1,0:T(2,128)(2,1)S(1)}, u32[]{:S(2)}, u32[]{:S(2)}) async-start(bf16[16,2,128]{2,1,0:T(2,128)(2,1)} %reshape.153), calls=%async_computation.1 | async-start | bytes 16384 | tf_op jit(solution)/shard_map/all_to_all | solution.py:69
  57.9 1.7 convolution_convert_fusion.3
  59.6 1.7 convolution_convert_fusion.2
  65.6 6.9 %all-to-all-start = ((bf16[16,2,128]{2,1,0:T(2,128)(2,1)}), bf16[16,2,128]{2,1,0:T(2,128)(2,1)S(1)}, u32[]{:S(2)}, u32[]{:S(2)}) async-start(bf16[16,2,128]{2,1,0:T(2,128)(2,1)} %reshape.149), calls=%async_computation | async-start | bytes 16384 | tf_op jit(solution)/shard_map/all_to_all | solution.py:68
  72.7 7.0 %all-to-all-done = bf16[16,2,128]{2,1,0:T(2,128)(2,1)S(1)} async-done(((bf16[16,2,128]{2,1,0:T(2,128)(2,1)}), bf16[16,2,128]{2,1,0:T(2,128)(2,1)S(1)}, u32[]{:S(2)}, u32[]{:S(2)}) %all-to-all-start) | async-done | bytes 8224 | tf_op jit(solution)/shard_map/all_to_all | solution.py:68
  79.7 3.5 %all-to-all-start.2 = ((bf16[16,2,256]{2,1,0:T(2,128)(2,1)}), bf16[16,2,256]{2,1,0:T(2,128)(2,1)S(1)}, u32[]{:S(2)}, u32[]{:S(2)}) async-start(bf16[16,2,256]{2,1,0:T(2,128)(2,1)} %reshape.151), calls=%async_computation.2 | async-start | bytes 32768 | tf_op jit(solution)/shard_map/all_to_all | solution.py:70
  84.5 6.1 %all-to-all-done.2 = bf16[16,2,256]{2,1,0:T(2,128)(2,1)S(1)} async-done(((bf16[16,2,256]{2,1,0:T(2,128)(2,1)}), bf16[16,2,256]{2,1,0:T(2,128)(2,1)S(1)}, u32[]{:S(2)}, u32[]{:S(2)}) %all-to-all-start.2) | async-done | bytes 16416 | tf_op jit(solution)/shard_map/all_to_all | solution.py:70
  90.6 3.5 %all-to-all-start.3 = ((bf16[16,2,256]{2,1,0:T(2,128)(2,1)}), bf16[16,2,256]{2,1,0:T(2,128)(2,1)S(1)}, u32[]{:S(2)}, u32[]{:S(2)}) async-start(bf16[16,2,256]{2,1,0:T(2,128)(2,1)} %reshape.155), calls=%async_computation.3 | async-start | bytes 32768 | tf_op jit(solution)/shard_map/all_to_all | solution.py:71
  94.3 4.2 %multiply_add_fusion = f32[4,4,256,512]{3,2,1,0:T(8,128)S(1)} fusion(f32[4,4,256,512]{3,2,1,0:T(8,128)} %param.20, f32[4,4,512]{2,1,0:T(4,128)S(1)} %reshape.121, f32[4,4,256]{2,1,0:T(4,128)S(1)} %reshape.120, f32[4,4]{1,0:T(4,128)S(1)} %subtract_exponential_fusion, f32[4,4]{1,0:T(4,128)S(1)} %get-tuple-element.6), kind=kLoop, calls=%fused_computation | loop fusion | flops 8388608 | bytes 16826496 | tf_op jit(solution)/shard_map/add | solution.py:81
  98.5 3.4 %copy-done.1 = f32[4,4,256,512]{3,2,1,0:T(8,128)} copy-done((f32[4,4,256,512]{3,2,1,0:T(8,128)}, f32[4,4,256,512]{3,2,1,0:T(8,128)S(1)}, u32[]{:S(2)}) %copy-start.1) | copy-done | bytes 8388632
  101.9 4.0 %fusion.30 = f32[4,4,1,512]{3,2,1,0:T(1,128)S(1)} fusion(f32[4,4,256,1]{2,3,1,0:T(1,128)S(1)} %reshape.141, f32[4,4,256,512]{3,2,1,0:T(8,128)S(1)} %multiply_add_fusion), kind=kOutput, calls=%fused_computation.57 | convolution fusion | flops 25165824 | bytes 8437760 | tf_op jit(solution)/shard_map/shd,shde->she/dot_general | solution.py:85
  106.1 6.9 %all-to-all-start.5 = ((f32[4,16,1]{0,2,1:T(1,128)}), f32[4,16,1]{0,2,1:T(1,128)S(1)}, u32[]{:S(2)}, u32[]{:S(2)}) async-start(f32[4,16,1]{0,2,1:T(1,128)} %copy.131), calls=%async_computation.5 | async-start | bytes 16384 | tf_op jit(solution)/shard_map/all_to_all | solution.py:109
  113.5 42.4 %all-gather.1 = bf16[16,4,2048]{2,1,0:T(4,128)(2,1)S(1)} all-gather(bf16[1,4,2048]{2,1,0:T(4,128)(2,1)S(1)} %fusion.25), channel_id=1, replica_groups=mesh['ep'=16,'tp'=2] {'ep'}, dimensions={0}, use_global_device_ids=true | all-gather | bytes 278528 | tf_op jit(solution)/shard_map/all_gather | solution.py:92
  157.9 4.0 %psum.7 = bf16[16,4,256]{2,1,0:T(4,128)(2,1)} all-reduce(bf16[16,4,256]{2,1,0:T(4,128)(2,1)S(1)} %all_to_all.24), channel_id=1, replica_groups=mesh['ep'=16,'tp'=2] {'tp'}, use_global_device_ids=true, to_apply=%region_2.3 | all-reduce | flops 16384 | bytes 65536 | tf_op jit(solution)/shard_map/psum | solution.py:93
  161.9 3.5 %all-to-all-start.4 = ((bf16[16,4,256]{2,1,0:T(4,128)(2,1)}), bf16[16,4,256]{2,1,0:T(4,128)(2,1)S(1)}, u32[]{:S(2)}, u32[]{:S(2)}) async-start(bf16[16,4,256]{2,1,0:T(4,128)(2,1)} %psum.7), calls=%async_computation.4 | async-start | bytes 65536 | tf_op jit(solution)/shard_map/all_to_all | solution.py:94
  165.5 7.3 %all-to-all-done.4 = bf16[16,4,256]{2,1,0:T(4,128)(2,1)S(1)} async-done(((bf16[16,4,256]{2,1,0:T(4,128)(2,1)}), bf16[16,4,256]{2,1,0:T(4,128)(2,1)S(1)}, u32[]{:S(2)}, u32[]{:S(2)}) %all-to-all-start.4) | async-done | bytes 32800 | tf_op jit(solution)/shard_map/all_to_all | solution.py:94
  173.0 39.4 %all-gather.2 = bf16[16,4,4096]{2,1,0:T(4,128)(2,1)S(1)} all-gather(bf16[1,4,4096]{2,1,0:T(4,128)(2,1)S(1)} %fusion.22), channel_id=1, replica_groups=mesh['ep'=16,'tp'=2] {'ep'}, dimensions={0}, use_global_device_ids=true | all-gather | bytes 557056 | tf_op jit(solution)/shard_map/all_gather | solution.py:99
  212.5 2.0 fusion.3
  214.6 3.8 %convolution_convert_fusion = bf16[64,4096]{1,0:T(8,128)(2,1)} fusion(bf16[1,256,4096]{2,1,0:T(8,128)(2,1)S(1)} %copy-done, bf16[64,4096]{1,0:T(8,128)(2,1)S(1)} %reshape.137, bf16[1,4096,256]{2,1,0:T(8,128)(2,1)} %param.34, f32[64,256]{1,0:T(8,128)S(1)} %fusion.3), kind=kOutput, calls=%fused_computation.1 | convolution fusion | flops 268795904 | bytes 5308416 | tf_op jit(solution)/shard_map/dot_general | solution.py:12
  219.6 1.9 reshape.118
  221.4 1.9 copy.132
  224.7 46.8 %all-reduce.2 = bf16[128,2048]{1,0:T(8,128)(2,1)S(1)} all-reduce(f32[128,2048]{1,0:T(8,128)} %reshape.119), channel_id=2, replica_groups=mesh['ep'=16,'tp'=2] {'ep','tp'}, use_global_device_ids=true, to_apply=%region_5.6.clone | all-reduce | flops 262144 | bytes 1572864
  271.5 1.8 all_gather.15
  (82 shorter events, 20.6 us)
Async XLA Ops:
  0.6 214.0 %copy-start = (bf16[1,256,4096]{2,1,0:T(8,128)(2,1)S(1)}, bf16[1,256,4096]{2,1,0:T(8,128)(2,1)}, u32[]{:S(2)}) copy-start(bf16[1,256,4096]{2,1,0:T(8,128)(2,1)} %param.35) | copy-start | bytes 6291460
  0.6 83.0 %copy-start.5 = (f32[4,4,256]{2,1,0:T(4,128)S(1)}, f32[4,4,256]{2,1,0:T(4,128)}, u32[]{:S(2)}) copy-start(f32[4,4,256]{2,1,0:T(4,128)} %param.21) | copy-start | bytes 49156
  50.3 15.3 %all-to-all-start.1 = ((bf16[16,2,128]{2,1,0:T(2,128)(2,1)}), bf16[16,2,128]{2,1,0:T(2,128)(2,1)S(1)}, u32[]{:S(2)}, u32[]{:S(2)}) async-start(bf16[16,2,128]{2,1,0:T(2,128)(2,1)} %reshape.153), calls=%async_computation.1 | async-start | bytes 16384 | tf_op jit(solution)/shard_map/all_to_all | solution.py:69
  56.5 42.0 %copy-start.6 = (f32[4,4]{1,0:T(4,128)}, f32[4,4]{1,0:T(4,128)S(1)}, u32[]{:S(2)}) copy-start(f32[4,4]{1,0:T(4,128)S(1)} %get-tuple-element.7) | copy-start | bytes 196
  65.6 14.1 %all-to-all-start = ((bf16[16,2,128]{2,1,0:T(2,128)(2,1)}), bf16[16,2,128]{2,1,0:T(2,128)(2,1)S(1)}, u32[]{:S(2)}, u32[]{:S(2)}) async-start(bf16[16,2,128]{2,1,0:T(2,128)(2,1)} %reshape.149), calls=%async_computation | async-start | bytes 16384 | tf_op jit(solution)/shard_map/all_to_all | solution.py:68
  79.7 10.9 %all-to-all-start.2 = ((bf16[16,2,256]{2,1,0:T(2,128)(2,1)}), bf16[16,2,256]{2,1,0:T(2,128)(2,1)S(1)}, u32[]{:S(2)}, u32[]{:S(2)}) async-start(bf16[16,2,256]{2,1,0:T(2,128)(2,1)} %reshape.151), calls=%async_computation.2 | async-start | bytes 32768 | tf_op jit(solution)/shard_map/all_to_all | solution.py:70
  90.6 15.5 %all-to-all-start.3 = ((bf16[16,2,256]{2,1,0:T(2,128)(2,1)}), bf16[16,2,256]{2,1,0:T(2,128)(2,1)S(1)}, u32[]{:S(2)}, u32[]{:S(2)}) async-start(bf16[16,2,256]{2,1,0:T(2,128)(2,1)} %reshape.155), calls=%async_computation.3 | async-start | bytes 32768 | tf_op jit(solution)/shard_map/all_to_all | solution.py:71
  98.5 3.4 %copy-start.1 = (f32[4,4,256,512]{3,2,1,0:T(8,128)}, f32[4,4,256,512]{3,2,1,0:T(8,128)S(1)}, u32[]{:S(2)}) copy-start(f32[4,4,256,512]{3,2,1,0:T(8,128)S(1)} %multiply_add_fusion) | copy-start | bytes 25165828
  101.9 54.7 %copy-start.3 = (bf16[2048,256]{1,0:T(8,128)(2,1)S(1)}, bf16[2048,256]{1,0:T(8,128)(2,1)}, u32[]{:S(2)}) copy-start(bf16[2048,256]{1,0:T(8,128)(2,1)} %param.31) | copy-start | bytes 3145732
  101.9 70.8 %copy-start.2 = (bf16[4,4096]{1,0:T(4,128)(2,1)S(1)}, bf16[4,4096]{1,0:T(4,128)(2,1)}, u32[]{:S(2)}) copy-start(bf16[4,4096]{1,0:T(4,128)(2,1)} %param.19) | copy-start | bytes 98308
  101.9 71.0 %copy-start.4 = (f32[4096]{0:T(1024)S(1)}, f32[4096]{0:T(1024)}, u32[]{:S(2)}) copy-start(f32[4096]{0:T(1024)} %param.32) | copy-start | bytes 49156
  106.1 55.8 %all-to-all-start.5 = ((f32[4,16,1]{0,2,1:T(1,128)}), f32[4,16,1]{0,2,1:T(1,128)S(1)}, u32[]{:S(2)}, u32[]{:S(2)}) async-start(f32[4,16,1]{0,2,1:T(1,128)} %copy.131), calls=%async_computation.5 | async-start | bytes 16384 | tf_op jit(solution)/shard_map/all_to_all | solution.py:109
  161.9 10.9 %all-to-all-start.4 = ((bf16[16,4,256]{2,1,0:T(4,128)(2,1)}), bf16[16,4,256]{2,1,0:T(4,128)(2,1)S(1)}, u32[]{:S(2)}, u32[]{:S(2)}) async-start(bf16[16,4,256]{2,1,0:T(4,128)(2,1)} %psum.7), calls=%async_computation.4 | async-start | bytes 65536 | tf_op jit(solution)/shard_map/all_to_all | solution.py:94
where the time goes:
time: 275 us; the launch traced here: 274 us
  blocking collectives  180 us (65%)
  starting transfers between devices  27.7 us (10%)
  waiting for transfers between devices  20.3 us (7%)
  matrix products  19 us (7%)
  local copies, waits for them, and re-layouts  15.6 us (6%)
  other arithmetic  10.7 us (4%)
    unnamed x1, blocking collectives  46.8 us
    all_gather x1, blocking collectives, body(): piece = lax.all_gather(normed, 'ep', axis=0, tiled=True)  45.3 us
    all_gather x1, blocking collectives, body(): lax.all_gather(hidden, 'ep', axis=0, tiled=True)  42.4 us
    all_gather x1, blocking collectives, body(): piece = lax.all_gather(ffn_in, 'ep', axis=0, tiled=True)  39.4 us
    dot_general x9, matrix products, product(): return jnp.dot(left, right, preferred_element_type=jnp.float32)  15 us
    unnamed x26, local copies, waits for them, and re-layouts  7.67 us
    all_to_all x1, waiting for transfers between devices, body(): lax.all_to_all(summed, 'ep', split_axis=0, concat_axis=1, tiled=True)  7.25 us
    all_to_all x1, waiting for transfers between devices, body(): lax.all_to_all(query_part, 'ep', split_axis=0, concat_axis=2, tiled=True)  6.95 us
  transfers between devices with their start and end apart: 6, of which 3 were waited for; matrix products, arithmetic and copies ran while one was open for 9% of the time, Pallas kernels for 0%

commit v1 on v0

--- a/solution.py
+++ b/solution.py
@@ -1,7 +1,25 @@
+import functools
 import jax
 import jax.numpy as jnp
 from jax import lax
 from jax.sharding import PartitionSpec as P
+
+
+def _view_surface(tile_in, named_axis, along_dim):
+    piece_now = lax.axis_size(named_axis)
+    reply = lax.axis_index(named_axis)
+    h_now, plain = (piece_now, reply)
+    step_out, far_arr = (tile_in, 1)
+    while far_arr < h_now:
+        later = lax.ppermute(step_out, named_axis, [(h, h ^ far_arr) for h in range(h_now)])
+        big = jnp.concatenate([step_out, later], along_dim)
+        even = jnp.concatenate([later, step_out], along_dim)
+        step_out = jnp.where(plain & far_arr == 0, big, even)
+        far_arr = 2 * far_arr
+    return step_out
+
+
+take_the_files = functools.partial(_view_surface, named_axis="ep", along_dim=0)
 
 
 def rms_scale(values, gain):
@@ -89,7 +107,7 @@
         hidden.reshape(seqs, value_width)
         * jax.nn.sigmoid(outgate.reshape(seqs, value_width).astype(jnp.float32))
     ).astype(jnp.bfloat16)
-    partial_value = product(lax.all_gather(hidden, "ep", axis=0, tiled=True), w_out)
+    partial_value = product(take_the_files(hidden), w_out)
     summed = lax.psum(rounded_term(partial_value).astype(jnp.bfloat16), "tp")
     mixed = lax.all_to_all(summed, "ep", split_axis=0, concat_axis=1, tiled=True)
     resid = tokens.astype(jnp.float32) + mixed.astype(jnp.float32)

time: 275 us -> 248 us (0.902)
  blocking collectives: 180 us -> 137 us
  waiting for transfers between devices: 20.3 us -> 28.6 us
  starting transfers between devices: 27.7 us -> 35.7 us
    all_gather x1 -> x0, blocking collectives: 42.4 us -> none  [body(): lax.all_gather(hidden, 'ep', axis=0, tiled=True)]
    ppermute x0 -> x4, starting transfers between devices: none -> 8.46 us  [_view_surface(): lax.ppermute(step_out, named_axis, [(h, h ^ far_arr) for h in range(h_now)])]
    ppermute x0 -> x4, waiting for transfers between devices: none -> 6.48 us  [_view_surface(): lax.ppermute(step_out, named_axis, [(h, h ^ far_arr) for h in range(h_now)])]
    unnamed x26 -> x27, local copies, waits for them, and re-layouts: 7.67 us -> 6.92 us
  transfers between devices with their start and end apart: 6 -> 10, of which waited for: 3 -> 7; matrix products, arithmetic and copies ran while one was open for 9% -> 9% of each run, Pallas kernels for 0% -> 0%
where the time goes in v1:
time: 248 us; the launch traced here: 247 us
  blocking collectives  137 us (55%)
  starting transfers between devices  35.7 us (14%)
  waiting for transfers between devices  28.6 us (12%)
  matrix products  19.3 us (8%)
  local copies, waits for them, and re-layouts  14.8 us (6%)
  other arithmetic  10 us (4%)
    unnamed x1, blocking collectives  47 us
    all_gather x1, blocking collectives, body(): piece = lax.all_gather(normed, 'ep', axis=0, tiled=True)  45.3 us
    all_gather x1, blocking collectives, body(): piece = lax.all_gather(ffn_in, 'ep', axis=0, tiled=True)  39.3 us
    dot_general x9, matrix products, product(): return jnp.dot(left, right, preferred_element_type=jnp.float32)  15.3 us
    ppermute x4, starting transfers between devices, _view_surface(): lax.ppermute(step_out, named_axis, [(h, h ^ far_arr) for h in range(h_now)])  8.46 us
    all_to_all x1, waiting for transfers between devices, body(): lax.all_to_all(summed, 'ep', split_axis=0, concat_axis=1, tiled=True)  7.28 us
    all_to_all x1, waiting for transfers between devices, body(): lax.all_to_all(query_part, 'ep', split_axis=0, concat_axis=2, tiled=True)  6.95 us
    unnamed x27, local copies, waits for them, and re-layouts  6.92 us
  transfers between devices with their start and end apart: 10, of which 7 were waited for; matrix products, arithmetic and copies ran while one was open for 9% of the time, Pallas kernels for 0%

profile of v1, /device:TPU:0, one launch (start us, length us, event | category | flops | bytes accessed | tf_op | source)
XLA Modules:
  0.0 246.9 jit_solution(17005531943680710488)
XLA Ops:
  2.6 45.3 %all-gather = bf16[16,4,4096]{2,1,0:T(4,128)(2,1)S(1)} all-gather(bf16[1,4,4096]{2,1,0:T(4,128)(2,1)S(1)} %fusion.54), channel_id=1, replica_groups=mesh['ep'=16,'tp'=2] {'ep'}, dimensions={0}, use_global_device_ids=true | all-gather | bytes 557056 | tf_op jit(solution)/shard_map/all_gather | solution.py:68
  50.3 3.5 %all-to-all-start.1 = ((bf16[16,2,128]{2,1,0:T(2,128)(2,1)}), bf16[16,2,128]{2,1,0:T(2,128)(2,1)S(1)}, u32[]{:S(2)}, u32[]{:S(2)}) async-start(bf16[16,2,128]{2,1,0:T(2,128)(2,1)} %reshape.151), calls=%async_computation.1 | async-start | bytes 16384 | tf_op jit(solution)/shard_map/all_to_all | solution.py:87
  64.1 6.9 %all-to-all-start = ((bf16[16,2,128]{2,1,0:T(2,128)(2,1)}), bf16[16,2,128]{2,1,0:T(2,128)(2,1)S(1)}, u32[]{:S(2)}, u32[]{:S(2)}) async-start(bf16[16,2,128]{2,1,0:T(2,128)(2,1)} %reshape.147), calls=%async_computation | async-start | bytes 16384 | tf_op jit(solution)/shard_map/all_to_all | solution.py:86
  71.3 7.0 %all-to-all-done = bf16[16,2,128]{2,1,0:T(2,128)(2,1)S(1)} async-done(((bf16[16,2,128]{2,1,0:T(2,128)(2,1)}), bf16[16,2,128]{2,1,0:T(2,128)(2,1)S(1)}, u32[]{:S(2)}, u32[]{:S(2)}) %all-to-all-start) | async-done | bytes 8224 | tf_op jit(solution)/shard_map/all_to_all | solution.py:86
  78.2 3.5 %all-to-all-start.2 = ((bf16[16,2,256]{2,1,0:T(2,128)(2,1)}), bf16[16,2,256]{2,1,0:T(2,128)(2,1)S(1)}, u32[]{:S(2)}, u32[]{:S(2)}) async-start(bf16[16,2,256]{2,1,0:T(2,128)(2,1)} %reshape.149), calls=%async_computation.2 | async-start | bytes 32768 | tf_op jit(solution)/shard_map/all_to_all | solution.py:88
  83.0 6.1 %all-to-all-done.2 = bf16[16,2,256]{2,1,0:T(2,128)(2,1)S(1)} async-done(((bf16[16,2,256]{2,1,0:T(2,128)(2,1)}), bf16[16,2,256]{2,1,0:T(2,128)(2,1)S(1)}, u32[]{:S(2)}, u32[]{:S(2)}) %all-to-all-start.2) | async-done | bytes 16416 | tf_op jit(solution)/shard_map/all_to_all | solution.py:88
  89.1 3.5 %all-to-all-start.3 = ((bf16[16,2,256]{2,1,0:T(2,128)(2,1)}), bf16[16,2,256]{2,1,0:T(2,128)(2,1)S(1)}, u32[]{:S(2)}, u32[]{:S(2)}) async-start(bf16[16,2,256]{2,1,0:T(2,128)(2,1)} %reshape.153), calls=%async_computation.3 | async-start | bytes 32768 | tf_op jit(solution)/shard_map/all_to_all | solution.py:89
  92.9 4.2 %multiply_add_fusion = f32[4,4,256,512]{3,2,1,0:T(8,128)S(1)} fusion(f32[4,4,256,512]{3,2,1,0:T(8,128)} %param.20, f32[4,4,512]{2,1,0:T(4,128)S(1)} %reshape.121, f32[4,4,256]{2,1,0:T(4,128)S(1)} %reshape.120, f32[4,4]{1,0:T(4,128)S(1)} %subtract_exponential_fusion, f32[4,4]{1,0:T(4,128)S(1)} %get-tuple-element.6), kind=kLoop, calls=%fused_computation | loop fusion | flops 8388608 | bytes 16826496 | tf_op jit(solution)/shard_map/add | solution.py:99
  97.1 3.4 %copy-done.1 = f32[4,4,256,512]{3,2,1,0:T(8,128)} copy-done((f32[4,4,256,512]{3,2,1,0:T(8,128)}, f32[4,4,256,512]{3,2,1,0:T(8,128)S(1)}, u32[]{:S(2)}) %copy-start.1) | copy-done | bytes 8388632
  100.5 4.0 %fusion.36 = f32[4,4,1,512]{3,2,1,0:T(1,128)S(1)} fusion(f32[4,4,256,1]{2,3,1,0:T(1,128)S(1)} %reshape.139, f32[4,4,256,512]{3,2,1,0:T(8,128)S(1)} %multiply_add_fusion), kind=kOutput, calls=%fused_computation.67 | convolution fusion | flops 25165824 | bytes 8437760 | tf_op jit(solution)/shard_map/shd,shde->she/dot_general | solution.py:103
  107.0 1.9 collective-permute-done
  110.9 2.1 collective-permute-done.1
  113.0 1.9 collective-permute-start.2
  114.9 2.4 collective-permute-done.2
  117.3 2.8 %collective-permute-start.3 = (bf16[32,2048]{1,0:T(8,128)(2,1)S(1)}, bf16[32,2048]{1,0:T(8,128)(2,1)S(1)}, u32[]{:S(2)}, u32[]{:S(2)}) collective-permute-start(bf16[32,2048]{1,0:T(8,128)(2,1)S(1)} %maximum_select_fusion.2), channel_id=1, source_target_pairs={{0,16},{2,18},{4,20},{6,22},{8,24},{10,26},{12,28},{14,30},{16,0},... | collective-permute-start | bytes 393224 | tf_op jit(solution)/shard_map/ppermute | solution.py:14
  120.9 4.7 %all-to-all-start.5 = ((f32[4,16,1]{0,2,1:T(1,128)}), f32[4,16,1]{0,2,1:T(1,128)S(1)}, u32[]{:S(2)}, u32[]{:S(2)}) async-start(f32[4,16,1]{0,2,1:T(1,128)} %copy.131), calls=%async_computation.5 | async-start | bytes 16384 | tf_op jit(solution)/shard_map/all_to_all | solution.py:127
  127.2 4.0 %psum.7 = bf16[16,4,256]{2,1,0:T(4,128)(2,1)} all-reduce(bf16[16,4,256]{2,1,0:T(4,128)(2,1)S(1)} %all_to_all.24), channel_id=1, replica_groups=mesh['ep'=16,'tp'=2] {'tp'}, use_global_device_ids=true, to_apply=%region_2.3 | all-reduce | flops 16384 | bytes 65536 | tf_op jit(solution)/shard_map/psum | solution.py:111
  133.0 5.2 %all-to-all-start.4 = ((bf16[16,4,256]{2,1,0:T(4,128)(2,1)}), bf16[16,4,256]{2,1,0:T(4,128)(2,1)S(1)}, u32[]{:S(2)}, u32[]{:S(2)}) async-start(bf16[16,4,256]{2,1,0:T(4,128)(2,1)} %psum.7), calls=%async_computation.4 | async-start | bytes 65536 | tf_op jit(solution)/shard_map/all_to_all | solution.py:112
  138.2 7.3 %all-to-all-done.4 = bf16[16,4,256]{2,1,0:T(4,128)(2,1)S(1)} async-done(((bf16[16,4,256]{2,1,0:T(4,128)(2,1)}), bf16[16,4,256]{2,1,0:T(4,128)(2,1)S(1)}, u32[]{:S(2)}, u32[]{:S(2)}) %all-to-all-start.4) | async-done | bytes 32800 | tf_op jit(solution)/shard_map/all_to_all | solution.py:112
  145.8 39.3 %all-gather.1 = bf16[16,4,4096]{2,1,0:T(4,128)(2,1)S(1)} all-gather(bf16[1,4,4096]{2,1,0:T(4,128)(2,1)S(1)} %fusion.28), channel_id=1, replica_groups=mesh['ep'=16,'tp'=2] {'ep'}, dimensions={0}, use_global_device_ids=true | all-gather | bytes 557056 | tf_op jit(solution)/shard_map/all_gather | solution.py:117
  185.2 2.0 fusion.3
  187.3 3.8 %convolution_convert_fusion = bf16[64,4096]{1,0:T(8,128)(2,1)} fusion(bf16[1,256,4096]{2,1,0:T(8,128)(2,1)S(1)} %copy-done, bf16[64,4096]{1,0:T(8,128)(2,1)S(1)} %reshape.135, bf16[1,4096,256]{2,1,0:T(8,128)(2,1)} %param.34, f32[64,256]{1,0:T(8,128)S(1)} %fusion.3), kind=kOutput, calls=%fused_computation.1 | convolution fusion | flops 268795904 | bytes 5308416 | tf_op jit(solution)/shard_map/dot_general | solution.py:30
  194.1 1.9 copy.132
  197.4 47.0 %all-reduce.2 = bf16[128,2048]{1,0:T(8,128)(2,1)S(1)} all-reduce(f32[128,2048]{1,0:T(8,128)} %reshape.119), channel_id=2, replica_groups=mesh['ep'=16,'tp'=2] {'ep','tp'}, use_global_device_ids=true, to_apply=%region_5.6.clone | all-reduce | flops 262144 | bytes 1572864
  (93 shorter events, 32.1 us)
Async XLA Ops:
  0.6 186.6 %copy-start = (bf16[1,256,4096]{2,1,0:T(8,128)(2,1)S(1)}, bf16[1,256,4096]{2,1,0:T(8,128)(2,1)}, u32[]{:S(2)}) copy-start(bf16[1,256,4096]{2,1,0:T(8,128)(2,1)} %param.35) | copy-start | bytes 6291460
  0.6 81.5 %copy-start.4 = (f32[4,4,256]{2,1,0:T(4,128)S(1)}, f32[4,4,256]{2,1,0:T(4,128)}, u32[]{:S(2)}) copy-start(f32[4,4,256]{2,1,0:T(4,128)} %param.21) | copy-start | bytes 49156
  50.3 13.8 %all-to-all-start.1 = ((bf16[16,2,128]{2,1,0:T(2,128)(2,1)}), bf16[16,2,128]{2,1,0:T(2,128)(2,1)S(1)}, u32[]{:S(2)}, u32[]{:S(2)}) async-start(bf16[16,2,128]{2,1,0:T(2,128)(2,1)} %reshape.151), calls=%async_computation.1 | async-start | bytes 16384 | tf_op jit(solution)/shard_map/all_to_all | solution.py:87
  61.3 35.8 %copy-start.5 = (f32[4,4]{1,0:T(4,128)}, f32[4,4]{1,0:T(4,128)S(1)}, u32[]{:S(2)}) copy-start(f32[4,4]{1,0:T(4,128)S(1)} %get-tuple-element.7) | copy-start | bytes 196
  64.1 14.1 %all-to-all-start = ((bf16[16,2,128]{2,1,0:T(2,128)(2,1)}), bf16[16,2,128]{2,1,0:T(2,128)(2,1)S(1)}, u32[]{:S(2)}, u32[]{:S(2)}) async-start(bf16[16,2,128]{2,1,0:T(2,128)(2,1)} %reshape.147), calls=%async_computation | async-start | bytes 16384 | tf_op jit(solution)/shard_map/all_to_all | solution.py:86
  78.2 10.9 %all-to-all-start.2 = ((bf16[16,2,256]{2,1,0:T(2,128)(2,1)}), bf16[16,2,256]{2,1,0:T(2,128)(2,1)S(1)}, u32[]{:S(2)}, u32[]{:S(2)}) async-start(bf16[16,2,256]{2,1,0:T(2,128)(2,1)} %reshape.149), calls=%async_computation.2 | async-start | bytes 32768 | tf_op jit(solution)/shard_map/all_to_all | solution.py:88
  89.1 15.5 %all-to-all-start.3 = ((bf16[16,2,256]{2,1,0:T(2,128)(2,1)}), bf16[16,2,256]{2,1,0:T(2,128)(2,1)S(1)}, u32[]{:S(2)}, u32[]{:S(2)}) async-start(bf16[16,2,256]{2,1,0:T(2,128)(2,1)} %reshape.153), calls=%async_computation.3 | async-start | bytes 32768 | tf_op jit(solution)/shard_map/all_to_all | solution.py:89
  97.1 3.4 %copy-start.1 = (f32[4,4,256,512]{3,2,1,0:T(8,128)}, f32[4,4,256,512]{3,2,1,0:T(8,128)S(1)}, u32[]{:S(2)}) copy-start(f32[4,4,256,512]{3,2,1,0:T(8,128)S(1)} %multiply_add_fusion) | copy-start | bytes 25165828
  100.5 19.7 %copy-start.6 = (f32[4,2]{0,1:T(2,128)S(1)}, f32[4,2]{0,1:T(2,128)}, u32[]{:S(2)}) copy-start(f32[4,2]{0,1:T(2,128)} %param.37) | copy-start | bytes 100
  100.5 19.7 %copy-start.7 = (s32[4,2]{0,1:T(2,128)S(1)}, s32[4,2]{0,1:T(2,128)}, u32[]{:S(2)}) copy-start(s32[4,2]{0,1:T(2,128)} %param.36) | copy-start | bytes 100
  100.5 45.1 %copy-start.2 = (bf16[4,4096]{1,0:T(4,128)(2,1)S(1)}, bf16[4,4096]{1,0:T(4,128)(2,1)}, u32[]{:S(2)}) copy-start(bf16[4,4096]{1,0:T(4,128)(2,1)} %param.19) | copy-start | bytes 98308
  100.5 45.2 %copy-start.3 = (f32[4096]{0:T(1024)S(1)}, f32[4096]{0:T(1024)}, u32[]{:S(2)}) copy-start(f32[4096]{0:T(1024)} %param.32) | copy-start | bytes 49156
  105.1 3.8 %collective-permute-start = (bf16[4,2048]{1,0:T(4,128)(2,1)S(1)}, bf16[4,2048]{1,0:T(4,128)(2,1)S(1)}, u32[]{:S(2)}, u32[]{:S(2)}) collective-permute-start(bf16[4,2048]{1,0:T(4,128)(2,1)S(1)} %multiply_convert_fusion.1), channel_id=1, source_target_pairs={{0,2},{2,0},{4,6},{6,4},{8,10},{10,8},{12,14},{14,12},{16,18},{18,... | collective-permute-start | bytes 49160 | tf_op jit(solution)/shard_map/ppermute | solution.py:14
  109.0 4.0 %collective-permute-start.1 = (bf16[8,2048]{1,0:T(8,128)(2,1)S(1)}, bf16[8,2048]{1,0:T(8,128)(2,1)S(1)}, u32[]{:S(2)}, u32[]{:S(2)}) collective-permute-start(bf16[8,2048]{1,0:T(8,128)(2,1)S(1)} %maximum_select_fusion.4), channel_id=1, source_target_pairs={{0,4},{2,6},{4,0},{6,2},{8,12},{10,14},{12,8},{14,10},{16,20},{18,... | collective-permute-start | bytes 98312 | tf_op jit(solution)/shard_map/ppermute | solution.py:14
  113.0 4.3 %collective-permute-start.2 = (bf16[16,2048]{1,0:T(8,128)(2,1)S(1)}, bf16[16,2048]{1,0:T(8,128)(2,1)S(1)}, u32[]{:S(2)}, u32[]{:S(2)}) collective-permute-start(bf16[16,2048]{1,0:T(8,128)(2,1)S(1)} %maximum_select_fusion.3), channel_id=1, source_target_pairs={{0,8},{2,10},{4,12},{6,14},{8,0},{10,2},{12,4},{14,6},{16,24},{18,... | collective-permute-start | bytes 196616 | tf_op jit(solution)/shard_map/ppermute | solution.py:14
  117.3 8.3 %collective-permute-start.3 = (bf16[32,2048]{1,0:T(8,128)(2,1)S(1)}, bf16[32,2048]{1,0:T(8,128)(2,1)S(1)}, u32[]{:S(2)}, u32[]{:S(2)}) collective-permute-start(bf16[32,2048]{1,0:T(8,128)(2,1)S(1)} %maximum_select_fusion.2), channel_id=1, source_target_pairs={{0,16},{2,18},{4,20},{6,22},{8,24},{10,26},{12,28},{14,30},{16,0},... | collective-permute-start | bytes 393224 | tf_op jit(solution)/shard_map/ppermute | solution.py:14
  120.9 12.0 %all-to-all-start.5 = ((f32[4,16,1]{0,2,1:T(1,128)}), f32[4,16,1]{0,2,1:T(1,128)S(1)}, u32[]{:S(2)}, u32[]{:S(2)}) async-start(f32[4,16,1]{0,2,1:T(1,128)} %copy.131), calls=%async_computation.5 | async-start | bytes 16384 | tf_op jit(solution)/shard_map/all_to_all | solution.py:127
  133.0 12.6 %all-to-all-start.4 = ((bf16[16,4,256]{2,1,0:T(4,128)(2,1)}), bf16[16,4,256]{2,1,0:T(4,128)(2,1)S(1)}, u32[]{:S(2)}, u32[]{:S(2)}) async-start(bf16[16,4,256]{2,1,0:T(4,128)(2,1)} %psum.7), calls=%async_computation.4 | async-start | bytes 65536 | tf_op jit(solution)/shard_map/all_to_all | solution.py:112
